TPU v7x, 32 devices: a whole 2x2x4 slice. The times are simulated.
32 devices in a mesh: sp: 4 (over y, x), tp: 8 (over z, core).
Axes of the slice: x: 2, y: 2, z: 4, core: 2. Of those that a mesh axis runs over, the one named last changes fastest.
Arguments:
- queries: bfloat16 [4096, 1024], P('sp', 'tp'), may hold values from -18 to 18
- keys: bfloat16 [4096, 256], P('sp'), may hold values from -18 to 18
- values: bfloat16 [4096, 256], P('sp'), may hold values from -6 to 6
- sink_logits: float32 [16], P('tp'), may hold values from 3 to 7
- w_out: bfloat16 [1024, 2048], P('tp'), may hold values from -1.5 to 1.5
- residual: bfloat16 [4096, 2048], P(('sp', 'tp')), may hold values from -6 to 6
- norm_gain: float32 [2048], replicated, may hold values from 0.1 to 1.9
- expert_ids: int32 [4096, 4], P('sp'), may hold values from 0 to 15, all different within a row; in each aligned block of 1024 rows (0 to 1023, 1024 to 2047, ...) at most 512 rows name the same one
- expert_weights: float32 [4096, 4], P('sp'), may hold values from 0.1 to 1.5
- w_gate: bfloat16 [32, 768, 2048], P(('sp', 'tp')), may hold values from -0.125 to 0.125
- w_up: bfloat16 [32, 768, 2048], P(('sp', 'tp')), may hold values from -0.125 to 0.125
- w_down: bfloat16 [32, 768, 2048], P(('sp', 'tp')), may hold values from -0.15625 to 0.15625
- shared_gate: bfloat16 [512, 2048], P('tp'), may hold values from -0.125 to 0.125
- shared_up: bfloat16 [512, 2048], P('tp'), may hold values from -0.125 to 0.125
- shared_down: bfloat16 [512, 2048], P('tp'), may hold values from -0.25 to 0.25
Outputs:
- layer_out: bfloat16 [4096, 2048], P(('sp', 'tp'))
Inputs may be any that keep to these rules, and one draw needn't show every extreme that they name: `expert_ids`: each row names 4 different experts; in each aligned block of 1024 rows no expert is named by more than 512 rows.
All inputs are finite; a program needn't handle non-finite values.
Results may differ from a plain program's by a relative error of at most 0.02.
Values may be sent and summed in bfloat16 or wider, within the bound.
No kernel may reach another device: no remote copies, remote signals or barrier semaphores. Data moves between devices by JAX's collectives and lax.ppermute only.
A program may use at most 128 MiB of HBM per device.

v0:
```python
import jax
import jax.numpy as jnp
from jax import lax
from jax.sharding import PartitionSpec as P

HD = 64
GROUP = 4
WINDOW = 128
TOPK = 4


def shifted(block, axis, distance):
    devices = range(lax.axis_size(axis))
    route = [(i - distance, i) for i in devices if i - distance in devices]
    return lax.ppermute(block, axis, route)


def from_partner(x, axis, apart):
    return lax.ppermute(x, axis, [(i, i ^ 1 << apart) for i in range(lax.axis_size(axis))])


def normalize(after_mix, norm_gain):
    values_f = after_mix.astype(jnp.float32)
    scale = lax.rsqrt(jnp.mean(values_f * values_f, axis=-1, keepdims=True) + 1e-06)
    return (values_f * scale * norm_gain).astype(jnp.bfloat16)


def slot_layout(route_ids, expert_count, capacity):
    flat_ids = route_ids.reshape(-1)
    matches = (flat_ids[:, None] == jnp.arange(expert_count, dtype=jnp.int32)[None, :]).astype(
        jnp.int32
    )
    earlier = jnp.cumsum(matches, axis=0) - matches
    order_in = jnp.sum(earlier * matches, axis=1)
    slot_index = flat_ids * capacity + order_in
    owners = jnp.arange(flat_ids.shape[0], dtype=jnp.int32) // TOPK
    slot_owner = jnp.full((expert_count * capacity,), -1, jnp.int32).at[slot_index].set(owners)
    return (slot_index, slot_owner)


def body(
    queries,
    keys,
    values,
    sink_logits,
    w_out,
    residual,
    norm_gain,
    expert_ids,
    expert_weights,
    w_gate,
    w_up,
    w_down,
    shared_gate,
    shared_up,
    shared_down,
):
    tp_count = lax.axis_size("tp")
    sp_count = lax.axis_size("sp")
    seq_rows = queries.shape[0]
    expert_count = sp_count * tp_count // 2
    capacity = max(2, 2 * seq_rows * TOPK // expert_count)
    local_heads = queries.shape[1] // HD
    kv_start = lax.axis_index("tp") * local_heads // GROUP * HD
    key_cols = lax.dynamic_slice_in_dim(keys, kv_start, HD, 1)
    value_cols = lax.dynamic_slice_in_dim(values, kv_start, HD, 1)
    rim_keys, rim_values = shifted(
        (key_cols[seq_rows - WINDOW :], value_cols[seq_rows - WINDOW :]), "sp", 1
    )
    num_blocks = seq_rows // WINDOW
    key_blocks = key_cols.reshape(num_blocks, WINDOW, HD)
    value_blocks = value_cols.reshape(num_blocks, WINDOW, HD)
    keys_ext = jnp.concatenate(
        [jnp.concatenate([rim_keys[None], key_blocks[:-1]], axis=0), key_blocks], axis=1
    )
    values_ext = jnp.concatenate(
        [jnp.concatenate([rim_values[None], value_blocks[:-1]], axis=0), value_blocks], axis=1
    )
    query_blocks = queries.reshape(num_blocks, WINDOW, local_heads, HD)
    scores = jnp.einsum(
        "nqhd,nsd->nhqs", query_blocks, keys_ext, preferred_element_type=jnp.float32
    ) * HD ** (-0.5)
    query_pos = jnp.arange(WINDOW)[:, None] + WINDOW
    key_pos = jnp.arange(2 * WINDOW)[None, :]
    in_band = (key_pos <= query_pos) & (key_pos > query_pos - WINDOW)
    absolute = (
        lax.axis_index("sp") * seq_rows
        + jnp.arange(num_blocks)[:, None, None] * WINDOW
        + key_pos[None]
        - WINDOW
    )
    allowed = in_band[None] & (absolute >= 0)
    scores = jnp.where(allowed[:, None], scores, -jnp.inf)
    sink_col = jnp.broadcast_to(sink_logits[None, :, None, None], scores.shape[:-1] + (1,))
    combined = jnp.concatenate([scores, sink_col], axis=-1)
    row_max = jnp.max(combined, axis=-1, keepdims=True)
    exps = jnp.exp(combined - row_max)
    weights = (exps[..., :-1] / jnp.sum(exps, axis=-1, keepdims=True)).astype(jnp.bfloat16)
    attended = jnp.einsum("nhqs,nsd->nqhd", weights, values_ext, preferred_element_type=jnp.float32)
    attended = attended.astype(jnp.bfloat16).reshape(seq_rows, local_heads * HD)
    head_rows = lax.all_to_all(attended, "tp", split_axis=0, concat_axis=1, tiled=True)
    projected = jnp.dot(
        head_rows,
        lax.all_gather(w_out, "tp", axis=0, tiled=True),
        preferred_element_type=jnp.float32,
    )
    after_mix = (residual.astype(jnp.float32) + projected).astype(jnp.bfloat16)
    normed = normalize(after_mix, norm_gain)
    tp_index = lax.axis_index("tp")
    lanes = tp_count // 2
    lane = tp_index // 2
    keep = tp_index % 2
    half_cap = capacity // 2
    slot_index, slot_owner = slot_layout(expert_ids, expert_count, capacity)
    all_rows = lax.all_gather(normed, "tp", axis=0, tiled=True)
    lane_owner = lax.dynamic_slice_in_dim(slot_owner.reshape(sp_count, lanes, capacity), lane, 1, 1)
    lane_owner = lane_owner.reshape(sp_count * capacity)
    picked = all_rows[jnp.maximum(lane_owner, 0)]
    outgoing = jnp.where((lane_owner >= 0)[:, None], picked, jnp.zeros((), jnp.bfloat16))
    arrived = lax.all_to_all(
        outgoing.reshape(sp_count, capacity, -1), "sp", split_axis=0, concat_axis=0, tiled=True
    )
    arrived = arrived.reshape(sp_count * capacity, -1)
    gate_act = jnp.einsum("td,fd->tf", arrived, w_gate[0], preferred_element_type=jnp.float32)
    up_act = jnp.einsum("td,fd->tf", arrived, w_up[0], preferred_element_type=jnp.float32)
    hidden = (jax.nn.silu(gate_act) * up_act).astype(jnp.bfloat16)
    half_out = jnp.dot(hidden, w_down[0], preferred_element_type=jnp.float32).astype(jnp.bfloat16)
    half_out = half_out.reshape(sp_count, 2, half_cap, -1)
    mine = lax.dynamic_index_in_dim(half_out, keep, 1, keepdims=False)
    other = lax.dynamic_index_in_dim(half_out, 1 - keep, 1, keepdims=False)
    partner = from_partner(other, "tp", 0)
    expert_sum = (mine.astype(jnp.float32) + partner.astype(jnp.float32)).astype(jnp.bfloat16)
    held = lax.all_to_all(expert_sum, "sp", split_axis=0, concat_axis=0, tiled=True).reshape(
        sp_count * half_cap, -1
    )
    route_rank = slot_index.reshape(seq_rows, TOPK) - expert_ids * capacity
    held_here = (expert_ids % lanes == lane) & (route_rank // half_cap == keep)
    position = expert_ids // lanes * half_cap + route_rank % half_cap
    scaled = jnp.where(held_here, expert_weights, jnp.zeros((), expert_weights.dtype))
    shared_gate_act = jnp.einsum(
        "td,fd->tf", all_rows, shared_gate, preferred_element_type=jnp.float32
    )
    shared_up_act = jnp.einsum("td,fd->tf", all_rows, shared_up, preferred_element_type=jnp.float32)
    shared_hidden = (jax.nn.silu(shared_gate_act) * shared_up_act).astype(jnp.bfloat16)
    partial_sum = jnp.dot(shared_hidden, shared_down, preferred_element_type=jnp.float32)
    for route_slot in range(TOPK):
        partial_sum = partial_sum + scaled[:, route_slot : route_slot + 1] * held[
            position[:, route_slot]
        ].astype(jnp.float32)
    moe_sum = lax.psum_scatter(
        partial_sum.astype(jnp.bfloat16), "tp", scatter_dimension=0, tiled=True
    )
    return (after_mix.astype(jnp.float32) + moe_sum.astype(jnp.float32)).astype(jnp.bfloat16)


def solution(mesh):
    return jax.shard_map(
        body,
        mesh=mesh,
        in_specs=(
            P("sp", "tp"),
            P("sp", None),
            P("sp", None),
            P("tp"),
            P("tp", None),
            P(("sp", "tp"), None),
            P(),
            P("sp", None),
            P("sp", None),
            P(("sp", "tp"), None, None),
            P(("sp", "tp"), None, None),
            P(("sp", "tp"), None, None),
            P("tp", None),
            P("tp", None),
            P("tp", None),
        ),
        out_specs=P(("sp", "tp"), None),
        check_vma=False,
    )
```

profile of v0, /device:TPU:0, one launch (start us, length us, event | category | flops | bytes accessed | tf_op | source)
XLA Modules:
  0.0 462.0 jit_solution(13587522794302528692)
XLA Ops:
  7.3 2.1 constant_dynamic-slice_fusion
  10.1 5.5 %collective-permute-start.1 = (bf16[128,64]{0,1:T(8,128)(2,1)}, bf16[128,64]{0,1:T(8,128)(2,1)}, u32[]{:S(2)}, u32[]{:S(2)}) collective-permute-start(bf16[128,64]{0,1:T(8,128)(2,1)} %slice.80), channel_id=1, source_target_pairs={{0,8},{8,16},{16,24},{1,9},{9,17},{17,25},{2,10},{10,18},{18,26},{... | collective-permute-start | bytes 49160 | tf_op jit(solution)/shard_map/ppermute | solution.py:15
  16.7 3.4 collective-permute-start
  22.7 2.0 reshape.266
  24.7 1.8 fusion.58
  28.0 21.9 %all_to_all.29 = bf16[8,128,128]{1,2,0:T(8,128)(2,1)S(1)} all-to-all(bf16[8,128,128]{1,2,0:T(8,128)(2,1)S(1)} %bitcast.99), channel_id=1, replica_groups=mesh['sp'=4,'tp'=8] {'tp'}, dimensions={0} | all-to-all | bytes 524288 | tf_op jit(solution)/shard_map/all_to_all | solution.py:101
  50.0 14.2 %all-gather.3.cloned.1.call-done = bf16[1024,2048]{1,0:T(8,128)(2,1)} async-done(((bf16[128,2048]{1,0:T(8,128)(2,1)}), bf16[1024,2048]{1,0:T(8,128)(2,1)}) %all-gather.3.cloned.1.call-update) | async-done | bytes 4194320 | tf_op jit(solution)/shard_map/all_gather | solution.py:104
  64.2 3.1 multiply_reduce_fusion
  73.8 8.3 %reduce-window.6 = s32[16,32,128]{2,1,0:T(8,128)S(1)} reduce-window(s32[16,32,128]{2,1,0:T(8,128)} %fusion.45, s32[]{:T(128)} %constant.127.clone.1), window={size=1x1x128 pad=0_0x0_0x127_0}, to_apply=%region_3.4 | reduce-window | flops 8323072 | bytes 524292 | tf_op jit(solution)/shard_map/reduce-window
  83.8 1.4 mul.144
  85.6 15.5 %scatter_custom_fusion = s32[8192]{0:T(1024)S(1)} fusion(s32[4096]{0:T(1024)S(1)} %bitcast.103, s32[4096]{0:T(1024)S(1)} %add_select_fusion.4, s32[]{:T(128)} %constant.132.clone.1), kind=kCustom, calls=%fused_computation.110 | custom fusion | bytes 32772 | tf_op jit(solution)/shard_map/scatter | solution.py:37
  101.2 13.8 %all-gather.5.cloned.1.call-done = bf16[1024,2048]{1,0:T(8,128)(2,1)} async-done(((bf16[128,2048]{1,0:T(8,128)(2,1)}), bf16[1024,2048]{1,0:T(8,128)(2,1)}) %all-gather.5.cloned.1.call-update) | async-done | bytes 4194320 | tf_op jit(solution)/shard_map/all_gather | solution.py:115
  115.0 19.0 %gather_fusion = bf16[2048,2048]{1,0:T(8,128)(2,1)} fusion(bf16[1024,2048]{1,0:T(8,128)(2,1)} %all-gather.5.cloned.1.call-done, s32[2048]{0:T(1024)S(1)} %broadcast_clamp_fusion), kind=kCustom, calls=%fused_computation | custom fusion | bytes 16785408 | tf_op jit(solution)/shard_map/gather | solution.py:118
  134.1 7.3 %broadcast_select_fusion = bf16[4,512,2048]{2,1,0:T(8,128)(2,1)} fusion(bf16[4,512,2048]{2,1,0:T(8,128)(2,1)} %bitcast.94, pred[4,512]{1,0:T(4,128)(4,1)S(1)} %bitcast.104), kind=kLoop, calls=%fused_computation.9 | loop fusion | flops 4194304 | bytes 16779264 | tf_op jit(solution)/shard_map/jit(_where)/select_n | solution.py:119
  141.3 5.9 %all-to-all-start.1 = ((bf16[4,512,2048]{2,1,0:T(8,128)(2,1)}), bf16[4,512,2048]{2,1,0:T(8,128)(2,1)}, u32[]{:S(2)}, u32[]{:S(2)}) async-start(bf16[4,512,2048]{2,1,0:T(8,128)(2,1)} %broadcast_select_fusion), calls=%async_computation.1 | async-start | bytes 16777216 | tf_op jit(solution)/shard_map/all_to_all | solution.py:120
  147.2 92.8 %all-to-all-done.1 = bf16[4,512,2048]{2,1,0:T(8,128)(2,1)} async-done(((bf16[4,512,2048]{2,1,0:T(8,128)(2,1)}), bf16[4,512,2048]{2,1,0:T(8,128)(2,1)}, u32[]{:S(2)}, u32[]{:S(2)}) %all-to-all-start.1) | async-done | bytes 8388640 | tf_op jit(solution)/shard_map/all_to_all | solution.py:120
  240.1 11.8 %fusion.4 = f32[2048,768]{1,0:T(8,128)} fusion(bf16[2048,2048]{1,0:T(8,128)(2,1)} %bitcast.16, bf16[1,768,2048]{2,1,0:T(8,128)(2,1)} %param.24), kind=kOutput, calls=%fused_computation.15 | convolution fusion | flops 6442450944 | bytes 17825792 | tf_op jit(solution)/shard_map/td,fd->tf/dot_general | solution.py:124
  251.8 21.3 %convolution_convert_fusion = bf16[2048,2048]{1,0:T(8,128)(2,1)} fusion(f32[2048,768]{1,0:T(8,128)} %fusion.4, bf16[2048,2048]{1,0:T(8,128)(2,1)} %bitcast.16, bf16[1,768,2048]{2,1,0:T(8,128)(2,1)S(1)} %copy-done, bf16[1,768,2048]{2,1,0:T(8,128)(2,1)} %param.25), kind=kOutput, calls=%fused_computation.10 | convolution fusion | flops 12898533376 | bytes 29360128 | tf_op jit(solution)/shard_map/dot_general | solution.py:127
  273.2 4.7 %dynamic-slice_bitcast_fusion = bf16[4,256,2048]{2,1,0:T(8,128)(2,1)} fusion(bf16[4,2,256,2048]{3,2,1,0:T(8,128)(2,1)} %bitcast.95, s32[]{:T(128)S(6)} %select_n.104), kind=kLoop, calls=%fused_computation.12 | loop fusion | bytes 8388612 | tf_op jit(solution)/shard_map/jit(dynamic_index_in_dim)/squeeze | solution.py:130
  277.9 7.5 %collective-permute-done.2 = bf16[4,256,2048]{2,1,0:T(8,128)(2,1)} collective-permute-done((bf16[4,256,2048]{2,1,0:T(8,128)(2,1)}, bf16[4,256,2048]{2,1,0:T(8,128)(2,1)}, u32[]{:S(2)}, u32[]{:S(2)}) %collective-permute-start.2) | collective-permute-done | bytes 4194336 | tf_op jit(solution)/shard_map/ppermute | solution.py:19
  285.4 7.7 %fusion = bf16[4,256,2048]{2,1,0:T(8,128)(2,1)} fusion(bf16[4,256,2048]{2,1,0:T(8,128)(2,1)} %collective-permute-done.2, bf16[4,2,256,2048]{3,2,1,0:T(8,128)(2,1)} %bitcast.96, s32[]{:T(128)S(6)} %select_n.103), kind=kLoop, calls=%fused_computation.7 | loop fusion | flops 8388608 | bytes 12582916 | tf_op jit(solution)/shard_map/convert_element_type | solution.py:132
  293.1 5.1 %all-to-all-start.2 = ((bf16[4,256,2048]{2,1,0:T(8,128)(2,1)}), bf16[4,256,2048]{2,1,0:T(8,128)(2,1)}, u32[]{:S(2)}, u32[]{:S(2)}) async-start(bf16[4,256,2048]{2,1,0:T(8,128)(2,1)} %fusion), calls=%async_computation.2 | async-start | bytes 8388608 | tf_op jit(solution)/shard_map/all_to_all | solution.py:133
  302.9 1.4 fusion.59
  304.3 8.0 %fusion.12 = f32[1024,2048]{1,0:T(8,128)} fusion(bf16[64,2048]{1,0:T(8,128)(2,1)S(1)} %copy-done.6, bf16[1024,2048]{1,0:T(8,128)(2,1)} %all-gather.5.cloned.1.call-done, bf16[64,2048]{1,0:T(8,128)(2,1)S(1)} %copy-done.7, f32[1024,64]{0,1:T(8,128)S(1)} %fusion.59), kind=kOutput, calls=%fused_computation.33 | convolution fusion | flops 537264128 | bytes 13369344 | tf_op jit(solution)/shard_map/dot_general | solution.py:145
  312.3 33.9 %all-to-all-done.2 = bf16[4,256,2048]{2,1,0:T(8,128)(2,1)} async-done(((bf16[4,256,2048]{2,1,0:T(8,128)(2,1)}), bf16[4,256,2048]{2,1,0:T(8,128)(2,1)}, u32[]{:S(2)}, u32[]{:S(2)}) %all-to-all-start.2) | async-done | bytes 4194336 | tf_op jit(solution)/shard_map/all_to_all | solution.py:133
  346.2 11.8 %gather_fusion.1 = bf16[1024,2048]{1,0:T(8,128)(2,1)} fusion(bf16[1024,2048]{1,0:T(8,128)(2,1)} %bitcast.23, s32[1024]{0:T(1024)S(1)} %get-tuple-element.24), kind=kCustom, calls=%fused_computation.1 | custom fusion | bytes 8392704 | tf_op jit(solution)/shard_map/gather | solution.py:147
  358.0 11.6 %gather_fusion.2 = bf16[1024,2048]{1,0:T(8,128)(2,1)} fusion(bf16[1024,2048]{1,0:T(8,128)(2,1)} %bitcast.23, s32[1024]{0:T(1024)S(1)} %get-tuple-element.23), kind=kCustom, calls=%fused_computation.2 | custom fusion | bytes 8392704 | tf_op jit(solution)/shard_map/gather | solution.py:147
  369.6 11.5 %gather_fusion.3 = bf16[1024,2048]{1,0:T(8,128)(2,1)} fusion(bf16[1024,2048]{1,0:T(8,128)(2,1)} %bitcast.23, s32[1024]{0:T(1024)S(1)} %get-tuple-element.22), kind=kCustom, calls=%fused_computation.3 | custom fusion | bytes 8392704 | tf_op jit(solution)/shard_map/gather | solution.py:147
  381.1 11.6 %gather_fusion.4 = bf16[1024,2048]{1,0:T(8,128)(2,1)} fusion(bf16[1024,2048]{1,0:T(8,128)(2,1)} %bitcast.23, s32[1024]{0:T(1024)S(1)} %get-tuple-element.21), kind=kCustom, calls=%fused_computation.4 | custom fusion | bytes 8392704 | tf_op jit(solution)/shard_map/gather | solution.py:147
  392.7 12.4 %add_convert_fusion = bf16[1024,2048]{1,0:T(8,128)(2,1)} fusion(bf16[1024,2048]{1,0:T(8,128)(2,1)} %gather_fusion.4, bf16[1024,2048]{1,0:T(8,128)(2,1)} %gather_fusion.3, bf16[1024,2048]{1,0:T(8,128)(2,1)} %gather_fusion.2, f32[1024,2048]{1,0:T(8,128)} %fusion.12, bf16[1024,2048]{1,0:T(8,128)(2,1)} %gather_fusion.1, f32[1024]{0:T(1024)S(1)} %get-tuple-element.6, ...), kind=kLoop, calls=%fused_computation.8 | loop fusion | flops 27262976 | bytes 29376512 | tf_op jit(solution)/shard_map/convert_element_type | solution.py:151
  405.1 48.2 %reduce-scatter.2.cloned.1.call-done = bf16[128,2048]{1,0:T(8,128)(2,1)} async-done(((bf16[1024,2048]{1,0:T(8,128)(2,1)}), bf16[128,2048]{1,0:T(8,128)(2,1)}) %reduce-scatter.2.cloned.1.call-update) | async-done | bytes 524304 | tf_op jit(solution)/shard_map/reduce_scatter | solution.py:150
  453.2 2.3 add_convert_fusion.1
  (81 shorter events, 19.7 us)
Async XLA Ops:
  6.5 245.3 %copy-start = (bf16[1,768,2048]{2,1,0:T(8,128)(2,1)S(1)}, bf16[1,768,2048]{2,1,0:T(8,128)(2,1)}, u32[]{:S(2)}) copy-start(bf16[1,768,2048]{2,1,0:T(8,128)(2,1)} %param.26) | copy-start | bytes 9437188
  6.5 57.6 %all-gather.3.cloned.1.call-start = ((), (), s32[]{:S(2)}) async-start(), calls=%async_computation.4 | async-start | bytes 4718592 | tf_op jit(solution)/shard_map/all_gather | solution.py:104
  7.3 107.8 %all-gather.5.cloned.1.call-start = ((), (), s32[]{:S(2)}) async-start(), calls=%async_computation.5 | async-start | bytes 4718592 | tf_op jit(solution)/shard_map/all_gather | solution.py:115
  10.1 14.5 %collective-permute-start.1 = (bf16[128,64]{0,1:T(8,128)(2,1)}, bf16[128,64]{0,1:T(8,128)(2,1)}, u32[]{:S(2)}, u32[]{:S(2)}) collective-permute-start(bf16[128,64]{0,1:T(8,128)(2,1)} %slice.80), channel_id=1, source_target_pairs={{0,8},{8,16},{16,24},{1,9},{9,17},{17,25},{2,10},{10,18},{18,26},{... | collective-permute-start | bytes 49160 | tf_op jit(solution)/shard_map/ppermute | solution.py:15
  16.7 10.3 %collective-permute-start = (bf16[128,64]{0,1:T(8,128)(2,1)S(1)}, bf16[128,64]{0,1:T(8,128)(2,1)}, u32[]{:S(2)}, u32[]{:S(2)}) collective-permute-start(bf16[128,64]{0,1:T(8,128)(2,1)S(1)} %slice.78), channel_id=1, source_target_pairs={{0,8},{8,16},{16,24},{1,9},{9,17},{17,25},{2,10},{10,18},{18,26},{... | collective-permute-start | bytes 49160 | tf_op jit(solution)/shard_map/ppermute | solution.py:15
  22.7 3.8 copy-start.12
  24.7 2.3 copy-start.9
  28.0 40.3 %copy-start.11 = (f32[2048]{0:T(1024)S(1)}, f32[2048]{0:T(1024)}, u32[]{:S(2)}) copy-start(f32[2048]{0:T(1024)} %param.21) | copy-start | bytes 24580
  50.0 19.4 %copy-start.8 = (s32[1024,4]{0,1:T(4,128)S(1)}, s32[1024,4]{0,1:T(4,128)}, u32[]{:S(2)}) copy-start(s32[1024,4]{0,1:T(4,128)} %param.22) | copy-start | bytes 49156
  67.3 1.1 copy-start.4
  141.3 98.7 %all-to-all-start.1 = ((bf16[4,512,2048]{2,1,0:T(8,128)(2,1)}), bf16[4,512,2048]{2,1,0:T(8,128)(2,1)}, u32[]{:S(2)}, u32[]{:S(2)}) async-start(bf16[4,512,2048]{2,1,0:T(8,128)(2,1)} %broadcast_select_fusion), calls=%async_computation.1 | async-start | bytes 16777216 | tf_op jit(solution)/shard_map/all_to_all | solution.py:120
  277.9 7.5 %collective-permute-start.2 = (bf16[4,256,2048]{2,1,0:T(8,128)(2,1)}, bf16[4,256,2048]{2,1,0:T(8,128)(2,1)}, u32[]{:S(2)}, u32[]{:S(2)}) collective-permute-start(bf16[4,256,2048]{2,1,0:T(8,128)(2,1)} %dynamic-slice_bitcast_fusion), channel_id=1, source_target_pairs={{0,1},{1,0},{2,3},{3,2},{4,5},{5,4},{6,7},{7,6},{8,9},{9,8},{10,11... | collective-permute-start | bytes 12582920 | tf_op jit(solution)/shard_map/ppermute | solution.py:19
  293.1 6.2 %copy-start.10 = (f32[1024,4]{0,1:T(4,128)S(1)}, f32[1024,4]{0,1:T(4,128)}, u32[]{:S(2)}) copy-start(f32[1024,4]{0,1:T(4,128)} %param.23) | copy-start | bytes 49156
  293.1 6.4 %copy-start.3 = (s32[1024,4]{1,0:T(8,128)S(1)}, s32[1024,4]{1,0:T(8,128)}, u32[]{:S(2)}) copy-start(s32[1024,4]{1,0:T(8,128)} %copy.50) | copy-start | bytes 49156
  293.1 53.1 %all-to-all-start.2 = ((bf16[4,256,2048]{2,1,0:T(8,128)(2,1)}), bf16[4,256,2048]{2,1,0:T(8,128)(2,1)}, u32[]{:S(2)}, u32[]{:S(2)}) async-start(bf16[4,256,2048]{2,1,0:T(8,128)(2,1)} %fusion), calls=%async_computation.2 | async-start | bytes 8388608 | tf_op jit(solution)/shard_map/all_to_all | solution.py:133
  298.2 155.0 %reduce-scatter.2.cloned.1.call-start = ((), (), s32[]{:S(2)}) async-start(), calls=%async_computation.6 | async-start | bytes 4718592 | tf_op jit(solution)/shard_map/reduce_scatter | solution.py:150
  299.6 3.3 copy-start.2
  299.6 3.3 copy-start.5
  301.8 2.5 copy-start.6
  301.8 2.5 copy-start.7
  392.7 62.8 %copy-start.1 = (bf16[1,768,2048]{2,1,0:T(8,128)(2,1)S(1)}, bf16[1,768,2048]{2,1,0:T(8,128)(2,1)}, u32[]{:S(2)}) copy-start(bf16[1,768,2048]{2,1,0:T(8,128)(2,1)} %param.26) | copy-start | bytes 9437188
Sparse Core Ops, SparseCore 0:
  8.9 55.1 all-gather.2
  69.5 45.5 all-gather.4
  405.2 47.9 reduce-scatter.1
where the time goes:
time: 464 us; the launch traced here: 462 us
  waiting for transfers between devices  211 us (45%)
  local copies, waits for them, and re-layouts  103 us (22%)
  matrix products  48.4 us (10%)
  other arithmetic  43.9 us (9%)
  blocking collectives  21.9 us (5%)
  starting transfers between devices  20.1 us (4%)
  between operations  13.5 us (3%)
    all_to_all x1, waiting for transfers between devices, body(): lax.all_to_all(outgoing.reshape(sp_count, capacity, -1), 'sp', split_axis...  92.8 us
    reduce_scatter x1, waiting for transfers between devices, body(): lax.psum_scatter(partial_sum.astype(jnp.bfloat16), 'tp', scatter_dimensio...  48.2 us
    gather x4, local copies, waits for them, and re-layouts, body(): held[position[:, route_slot]].astype(jnp.float32)  46.5 us
    all_to_all x1, waiting for transfers between devices, body(): lax.all_to_all(expert_sum, 'sp', split_axis=0, concat_axis=0, tiled=True)  33.9 us
    all_to_all x1, blocking collectives, body(): lax.all_to_all(attended, 'tp', split_axis=0, concat_axis=1, tiled=True)  21.9 us
    dot_general x1, matrix products, body(): jnp.dot(hidden, w_down[0], preferred_element_type=jnp.float32)  21.3 us
    gather x1, local copies, waits for them, and re-layouts, body(): picked = all_rows[jnp.maximum(lane_owner, 0)]  19 us
    scatter x1, local copies, waits for them, and re-layouts, slot_layout(): jnp.full((expert_count * capacity,), -1, jnp.int32).at[slot_index]  15.5 us
  transfers between devices with their start and end apart: 8, of which 6 were waited for; matrix products, arithmetic and copies ran while one was open for 12% of the time, Pallas kernels for 0%

commit v1 on v0

--- a/solution.py
+++ b/solution.py
@@ -98,7 +98,19 @@
     weights = (exps[..., :-1] / jnp.sum(exps, axis=-1, keepdims=True)).astype(jnp.bfloat16)
     attended = jnp.einsum("nhqs,nsd->nqhd", weights, values_ext, preferred_element_type=jnp.float32)
     attended = attended.astype(jnp.bfloat16).reshape(seq_rows, local_heads * HD)
-    head_rows = lax.all_to_all(attended, "tp", split_axis=0, concat_axis=1, tiled=True)
+
+    def list_matrix_in(xs):
+        return jnp.concatenate(
+            lax.all_to_all(
+                jnp.stack(jnp.split(xs, lax.axis_size("tp"), axis=0), axis=0),
+                axis_name="tp",
+                split_axis=0,
+                concat_axis=0,
+            ),
+            axis=1,
+        )
+
+    head_rows = list_matrix_in(attended)
     projected = jnp.dot(
         head_rows,
         lax.all_gather(w_out, "tp", axis=0, tiled=True),

time: 464 us -> 464 us (level)
  no operation moved by 1% of the time
where the time goes in v1:
time: 464 us; the launch traced here: 462 us
  waiting for transfers between devices  211 us (45%)
  local copies, waits for them, and re-layouts  103 us (22%)
  matrix products  48.4 us (10%)
  other arithmetic  43.9 us (9%)
  blocking collectives  21.9 us (5%)
  starting transfers between devices  20.1 us (4%)
  between operations  13.6 us (3%)
    all_to_all x1, waiting for transfers between devices, body(): lax.all_to_all(outgoing.reshape(sp_count, capacity, -1), 'sp', split_axis...  92.8 us
    reduce_scatter x1, waiting for transfers between devices, body(): lax.psum_scatter(partial_sum.astype(jnp.bfloat16), 'tp', scatter_dimensio...  48.2 us
    gather x4, local copies, waits for them, and re-layouts, body(): held[position[:, route_slot]].astype(jnp.float32)  46.5 us
    all_to_all x1, waiting for transfers between devices, body(): lax.all_to_all(expert_sum, 'sp', split_axis=0, concat_axis=0, tiled=True)  33.9 us
    all_to_all x1, blocking collectives, list_matrix_in(): lax.all_to_all(jnp.stack(jnp.split(xs, lax.axis_size('tp'), axis=0), axis...  21.9 us
    dot_general x1, matrix products, body(): jnp.dot(hidden, w_down[0], preferred_element_type=jnp.float32)  21.3 us
    gather x1, local copies, waits for them, and re-layouts, body(): picked = all_rows[jnp.maximum(lane_owner, 0)]  19 us
    scatter x1, local copies, waits for them, and re-layouts, slot_layout(): jnp.full((expert_count * capacity,), -1, jnp.int32).at[slot_index]  15.5 us
  transfers between devices with their start and end apart: 8, of which 6 were waited for; matrix products, arithmetic and copies ran while one was open for 12% of the time, Pallas kernels for 0%

profile of v1, /device:TPU:0, one launch (start us, length us, event | category | flops | bytes accessed | tf_op | source)
XLA Modules:
  0.0 462.0 jit_solution(2828358751631203110)
XLA Ops:
  7.3 2.1 constant_dynamic-slice_fusion
  10.1 5.5 %collective-permute-start.1 = (bf16[128,64]{0,1:T(8,128)(2,1)}, bf16[128,64]{0,1:T(8,128)(2,1)}, u32[]{:S(2)}, u32[]{:S(2)}) collective-permute-start(bf16[128,64]{0,1:T(8,128)(2,1)} %slice.88), channel_id=1, source_target_pairs={{0,8},{8,16},{16,24},{1,9},{9,17},{17,25},{2,10},{10,18},{18,26},{... | collective-permute-start | bytes 49160 | tf_op jit(solution)/shard_map/ppermute | solution.py:15
  16.7 3.4 collective-permute-start
  22.7 2.0 reshape.286
  24.7 1.8 fusion.60
  28.2 21.9 %all_to_all.15 = bf16[8,128,128]{1,2,0:T(8,128)(2,1)S(1)} all-to-all(bf16[8,128,128]{1,2,0:T(8,128)(2,1)S(1)} %constant_dynamic-update-slice_fusion), channel_id=1, replica_groups=mesh['sp'=4,'tp'=8] {'tp'}, dimensions={0} | all-to-all | bytes 524288 | tf_op jit(solution)/shard_map/all_to_all | solution.py:104
  50.1 14.1 %all-gather.3.cloned.1.call-done = bf16[1024,2048]{1,0:T(8,128)(2,1)} async-done(((bf16[128,2048]{1,0:T(8,128)(2,1)}), bf16[1024,2048]{1,0:T(8,128)(2,1)}) %all-gather.3.cloned.1.call-update) | async-done | bytes 4194320 | tf_op jit(solution)/shard_map/all_gather | solution.py:116
  64.2 3.1 multiply_reduce_fusion
  73.8 8.3 %reduce-window.6 = s32[16,32,128]{2,1,0:T(8,128)S(1)} reduce-window(s32[16,32,128]{2,1,0:T(8,128)} %fusion.46, s32[]{:T(128)} %constant.127.clone.1), window={size=1x1x128 pad=0_0x0_0x127_0}, to_apply=%region_3.4 | reduce-window | flops 8323072 | bytes 524292 | tf_op jit(solution)/shard_map/reduce-window
  83.8 1.4 mul.144
  85.6 15.5 %scatter_custom_fusion = s32[8192]{0:T(1024)S(1)} fusion(s32[4096]{0:T(1024)S(1)} %bitcast.117, s32[4096]{0:T(1024)S(1)} %add_select_fusion.4, s32[]{:T(128)} %constant.132.clone.1), kind=kCustom, calls=%fused_computation.119 | custom fusion | bytes 32772 | tf_op jit(solution)/shard_map/scatter | solution.py:37
  101.2 13.8 %all-gather.5.cloned.1.call-done = bf16[1024,2048]{1,0:T(8,128)(2,1)} async-done(((bf16[128,2048]{1,0:T(8,128)(2,1)}), bf16[1024,2048]{1,0:T(8,128)(2,1)}) %all-gather.5.cloned.1.call-update) | async-done | bytes 4194320 | tf_op jit(solution)/shard_map/all_gather | solution.py:127
  115.0 19.0 %gather_fusion = bf16[2048,2048]{1,0:T(8,128)(2,1)} fusion(bf16[1024,2048]{1,0:T(8,128)(2,1)} %all-gather.5.cloned.1.call-done, s32[2048]{0:T(1024)S(1)} %broadcast_clamp_fusion), kind=kCustom, calls=%fused_computation | custom fusion | bytes 16785408 | tf_op jit(solution)/shard_map/gather | solution.py:130
  134.1 7.3 %broadcast_select_fusion = bf16[4,512,2048]{2,1,0:T(8,128)(2,1)} fusion(bf16[4,512,2048]{2,1,0:T(8,128)(2,1)} %bitcast.101, pred[4,512]{1,0:T(4,128)(4,1)S(1)} %bitcast.118), kind=kLoop, calls=%fused_computation.9 | loop fusion | flops 4194304 | bytes 16779264 | tf_op jit(solution)/shard_map/jit(_where)/select_n | solution.py:131
  141.3 5.9 %all-to-all-start.1 = ((bf16[4,512,2048]{2,1,0:T(8,128)(2,1)}), bf16[4,512,2048]{2,1,0:T(8,128)(2,1)}, u32[]{:S(2)}, u32[]{:S(2)}) async-start(bf16[4,512,2048]{2,1,0:T(8,128)(2,1)} %broadcast_select_fusion), calls=%async_computation.1 | async-start | bytes 16777216 | tf_op jit(solution)/shard_map/all_to_all | solution.py:132
  147.2 92.8 %all-to-all-done.1 = bf16[4,512,2048]{2,1,0:T(8,128)(2,1)} async-done(((bf16[4,512,2048]{2,1,0:T(8,128)(2,1)}), bf16[4,512,2048]{2,1,0:T(8,128)(2,1)}, u32[]{:S(2)}, u32[]{:S(2)}) %all-to-all-start.1) | async-done | bytes 8388640 | tf_op jit(solution)/shard_map/all_to_all | solution.py:132
  240.1 11.8 %fusion.4 = f32[2048,768]{1,0:T(8,128)} fusion(bf16[2048,2048]{1,0:T(8,128)(2,1)} %bitcast.23, bf16[1,768,2048]{2,1,0:T(8,128)(2,1)} %param.24), kind=kOutput, calls=%fused_computation.15 | convolution fusion | flops 6442450944 | bytes 17825792 | tf_op jit(solution)/shard_map/td,fd->tf/dot_general | solution.py:136
  251.8 21.3 %convolution_convert_fusion = bf16[2048,2048]{1,0:T(8,128)(2,1)} fusion(f32[2048,768]{1,0:T(8,128)} %fusion.4, bf16[2048,2048]{1,0:T(8,128)(2,1)} %bitcast.23, bf16[1,768,2048]{2,1,0:T(8,128)(2,1)S(1)} %copy-done, bf16[1,768,2048]{2,1,0:T(8,128)(2,1)} %param.25), kind=kOutput, calls=%fused_computation.10 | convolution fusion | flops 12898533376 | bytes 29360128 | tf_op jit(solution)/shard_map/dot_general | solution.py:139
  273.2 4.7 %dynamic-slice_bitcast_fusion = bf16[4,256,2048]{2,1,0:T(8,128)(2,1)} fusion(bf16[4,2,256,2048]{3,2,1,0:T(8,128)(2,1)} %bitcast.102, s32[]{:T(128)S(6)} %select_n.104), kind=kLoop, calls=%fused_computation.12 | loop fusion | bytes 8388612 | tf_op jit(solution)/shard_map/jit(dynamic_index_in_dim)/squeeze | solution.py:142
  277.9 7.5 %collective-permute-done.2 = bf16[4,256,2048]{2,1,0:T(8,128)(2,1)} collective-permute-done((bf16[4,256,2048]{2,1,0:T(8,128)(2,1)}, bf16[4,256,2048]{2,1,0:T(8,128)(2,1)}, u32[]{:S(2)}, u32[]{:S(2)}) %collective-permute-start.2) | collective-permute-done | bytes 4194336 | tf_op jit(solution)/shard_map/ppermute | solution.py:19
  285.4 7.7 %fusion = bf16[4,256,2048]{2,1,0:T(8,128)(2,1)} fusion(bf16[4,256,2048]{2,1,0:T(8,128)(2,1)} %collective-permute-done.2, bf16[4,2,256,2048]{3,2,1,0:T(8,128)(2,1)} %bitcast.103, s32[]{:T(128)S(6)} %select_n.103), kind=kLoop, calls=%fused_computation.7 | loop fusion | flops 8388608 | bytes 12582916 | tf_op jit(solution)/shard_map/convert_element_type | solution.py:144
  293.1 5.1 %all-to-all-start.2 = ((bf16[4,256,2048]{2,1,0:T(8,128)(2,1)}), bf16[4,256,2048]{2,1,0:T(8,128)(2,1)}, u32[]{:S(2)}, u32[]{:S(2)}) async-start(bf16[4,256,2048]{2,1,0:T(8,128)(2,1)} %fusion), calls=%async_computation.2 | async-start | bytes 8388608 | tf_op jit(solution)/shard_map/all_to_all | solution.py:145
  302.9 1.4 fusion.61
  304.3 8.0 %fusion.13 = f32[1024,2048]{1,0:T(8,128)} fusion(bf16[64,2048]{1,0:T(8,128)(2,1)S(1)} %copy-done.6, bf16[1024,2048]{1,0:T(8,128)(2,1)} %all-gather.5.cloned.1.call-done, bf16[64,2048]{1,0:T(8,128)(2,1)S(1)} %copy-done.7, f32[1024,64]{0,1:T(8,128)S(1)} %fusion.61), kind=kOutput, calls=%fused_computation.34 | convolution fusion | flops 537264128 | bytes 13369344 | tf_op jit(solution)/shard_map/dot_general | solution.py:157
  312.3 33.9 %all-to-all-done.2 = bf16[4,256,2048]{2,1,0:T(8,128)(2,1)} async-done(((bf16[4,256,2048]{2,1,0:T(8,128)(2,1)}), bf16[4,256,2048]{2,1,0:T(8,128)(2,1)}, u32[]{:S(2)}, u32[]{:S(2)}) %all-to-all-start.2) | async-done | bytes 4194336 | tf_op jit(solution)/shard_map/all_to_all | solution.py:145
  346.2 11.8 %gather_fusion.1 = bf16[1024,2048]{1,0:T(8,128)(2,1)} fusion(bf16[1024,2048]{1,0:T(8,128)(2,1)} %bitcast.30, s32[1024]{0:T(1024)S(1)} %get-tuple-element.32), kind=kCustom, calls=%fused_computation.1 | custom fusion | bytes 8392704 | tf_op jit(solution)/shard_map/gather | solution.py:159
  358.0 11.6 %gather_fusion.2 = bf16[1024,2048]{1,0:T(8,128)(2,1)} fusion(bf16[1024,2048]{1,0:T(8,128)(2,1)} %bitcast.30, s32[1024]{0:T(1024)S(1)} %get-tuple-element.31), kind=kCustom, calls=%fused_computation.2 | custom fusion | bytes 8392704 | tf_op jit(solution)/shard_map/gather | solution.py:159
  369.6 11.5 %gather_fusion.3 = bf16[1024,2048]{1,0:T(8,128)(2,1)} fusion(bf16[1024,2048]{1,0:T(8,128)(2,1)} %bitcast.30, s32[1024]{0:T(1024)S(1)} %get-tuple-element.30), kind=kCustom, calls=%fused_computation.3 | custom fusion | bytes 8392704 | tf_op jit(solution)/shard_map/gather | solution.py:159
  381.1 11.6 %gather_fusion.4 = bf16[1024,2048]{1,0:T(8,128)(2,1)} fusion(bf16[1024,2048]{1,0:T(8,128)(2,1)} %bitcast.30, s32[1024]{0:T(1024)S(1)} %get-tuple-element.29), kind=kCustom, calls=%fused_computation.4 | custom fusion | bytes 8392704 | tf_op jit(solution)/shard_map/gather | solution.py:159
  392.7 12.4 %add_convert_fusion = bf16[1024,2048]{1,0:T(8,128)(2,1)} fusion(bf16[1024,2048]{1,0:T(8,128)(2,1)} %gather_fusion.4, bf16[1024,2048]{1,0:T(8,128)(2,1)} %gather_fusion.3, bf16[1024,2048]{1,0:T(8,128)(2,1)} %gather_fusion.2, f32[1024,2048]{1,0:T(8,128)} %fusion.13, bf16[1024,2048]{1,0:T(8,128)(2,1)} %gather_fusion.1, f32[1024]{0:T(1024)S(1)} %get-tuple-element.6, ...), kind=kLoop, calls=%fused_computation.8 | loop fusion | flops 27262976 | bytes 29376512 | tf_op jit(solution)/shard_map/convert_element_type | solution.py:163
  405.1 48.2 %reduce-scatter.2.cloned.1.call-done = bf16[128,2048]{1,0:T(8,128)(2,1)} async-done(((bf16[1024,2048]{1,0:T(8,128)(2,1)}), bf16[128,2048]{1,0:T(8,128)(2,1)}) %reduce-scatter.2.cloned.1.call-update) | async-done | bytes 524304 | tf_op jit(solution)/shard_map/reduce_scatter | solution.py:162
  453.2 2.3 add_convert_fusion.1
  (90 shorter events, 19.8 us)
Async XLA Ops:
  6.5 245.3 %copy-start = (bf16[1,768,2048]{2,1,0:T(8,128)(2,1)S(1)}, bf16[1,768,2048]{2,1,0:T(8,128)(2,1)}, u32[]{:S(2)}) copy-start(bf16[1,768,2048]{2,1,0:T(8,128)(2,1)} %param.26) | copy-start | bytes 9437188
  6.5 57.6 %all-gather.3.cloned.1.call-start = ((), (), s32[]{:S(2)}) async-start(), calls=%async_computation.4 | async-start | bytes 4718592 | tf_op jit(solution)/shard_map/all_gather | solution.py:116
  7.3 107.8 %all-gather.5.cloned.1.call-start = ((), (), s32[]{:S(2)}) async-start(), calls=%async_computation.5 | async-start | bytes 4718592 | tf_op jit(solution)/shard_map/all_gather | solution.py:127
  10.1 14.5 %collective-permute-start.1 = (bf16[128,64]{0,1:T(8,128)(2,1)}, bf16[128,64]{0,1:T(8,128)(2,1)}, u32[]{:S(2)}, u32[]{:S(2)}) collective-permute-start(bf16[128,64]{0,1:T(8,128)(2,1)} %slice.88), channel_id=1, source_target_pairs={{0,8},{8,16},{16,24},{1,9},{9,17},{17,25},{2,10},{10,18},{18,26},{... | collective-permute-start | bytes 49160 | tf_op jit(solution)/shard_map/ppermute | solution.py:15
  16.7 10.3 %collective-permute-start = (bf16[128,64]{0,1:T(8,128)(2,1)S(1)}, bf16[128,64]{0,1:T(8,128)(2,1)}, u32[]{:S(2)}, u32[]{:S(2)}) collective-permute-start(bf16[128,64]{0,1:T(8,128)(2,1)S(1)} %slice.86), channel_id=1, source_target_pairs={{0,8},{8,16},{16,24},{1,9},{9,17},{17,25},{2,10},{10,18},{18,26},{... | collective-permute-start | bytes 49160 | tf_op jit(solution)/shard_map/ppermute | solution.py:15
  22.7 3.8 copy-start.12
  24.7 2.3 copy-start.9
  28.0 40.3 %copy-start.11 = (f32[2048]{0:T(1024)S(1)}, f32[2048]{0:T(1024)}, u32[]{:S(2)}) copy-start(f32[2048]{0:T(1024)} %param.21) | copy-start | bytes 24580
  50.1 19.2 %copy-start.8 = (s32[1024,4]{0,1:T(4,128)S(1)}, s32[1024,4]{0,1:T(4,128)}, u32[]{:S(2)}) copy-start(s32[1024,4]{0,1:T(4,128)} %param.22) | copy-start | bytes 49156
  67.3 1.1 copy-start.4
  141.3 98.7 %all-to-all-start.1 = ((bf16[4,512,2048]{2,1,0:T(8,128)(2,1)}), bf16[4,512,2048]{2,1,0:T(8,128)(2,1)}, u32[]{:S(2)}, u32[]{:S(2)}) async-start(bf16[4,512,2048]{2,1,0:T(8,128)(2,1)} %broadcast_select_fusion), calls=%async_computation.1 | async-start | bytes 16777216 | tf_op jit(solution)/shard_map/all_to_all | solution.py:132
  277.9 7.5 %collective-permute-start.2 = (bf16[4,256,2048]{2,1,0:T(8,128)(2,1)}, bf16[4,256,2048]{2,1,0:T(8,128)(2,1)}, u32[]{:S(2)}, u32[]{:S(2)}) collective-permute-start(bf16[4,256,2048]{2,1,0:T(8,128)(2,1)} %dynamic-slice_bitcast_fusion), channel_id=1, source_target_pairs={{0,1},{1,0},{2,3},{3,2},{4,5},{5,4},{6,7},{7,6},{8,9},{9,8},{10,11... | collective-permute-start | bytes 12582920 | tf_op jit(solution)/shard_map/ppermute | solution.py:19
  293.1 6.2 %copy-start.10 = (f32[1024,4]{0,1:T(4,128)S(1)}, f32[1024,4]{0,1:T(4,128)}, u32[]{:S(2)}) copy-start(f32[1024,4]{0,1:T(4,128)} %param.23) | copy-start | bytes 49156
  293.1 6.4 %copy-start.3 = (s32[1024,4]{1,0:T(8,128)S(1)}, s32[1024,4]{1,0:T(8,128)}, u32[]{:S(2)}) copy-start(s32[1024,4]{1,0:T(8,128)} %copy.50) | copy-start | bytes 49156
  293.1 53.1 %all-to-all-start.2 = ((bf16[4,256,2048]{2,1,0:T(8,128)(2,1)}), bf16[4,256,2048]{2,1,0:T(8,128)(2,1)}, u32[]{:S(2)}, u32[]{:S(2)}) async-start(bf16[4,256,2048]{2,1,0:T(8,128)(2,1)} %fusion), calls=%async_computation.2 | async-start | bytes 8388608 | tf_op jit(solution)/shard_map/all_to_all | solution.py:145
  298.2 155.0 %reduce-scatter.2.cloned.1.call-start = ((), (), s32[]{:S(2)}) async-start(), calls=%async_computation.6 | async-start | bytes 4718592 | tf_op jit(solution)/shard_map/reduce_scatter | solution.py:162
  299.6 3.3 copy-start.2
  299.6 3.3 copy-start.5
  301.8 2.5 copy-start.6
  301.8 2.5 copy-start.7
  392.7 62.8 %copy-start.1 = (bf16[1,768,2048]{2,1,0:T(8,128)(2,1)S(1)}, bf16[1,768,2048]{2,1,0:T(8,128)(2,1)}, u32[]{:S(2)}) copy-start(bf16[1,768,2048]{2,1,0:T(8,128)(2,1)} %param.26) | copy-start | bytes 9437188
Sparse Core Ops, SparseCore 0:
  8.9 55.1 all-gather.2
  69.5 45.5 all-gather.4
  405.2 47.9 reduce-scatter.1
